TPU v7x, 512 devices: a 4x2x32 block of a 4x8x32 slice. The times are simulated.
512 devices in a mesh: grp: 2 (over y), kv: 32 (over z), tp: 8 (over x, core).
Axes of the slice: x: 4, y: 2, z: 32, core: 2. Of those that a mesh axis runs over, the one named last changes fastest.
The devices are a block of a 4x8x32 slice.
Arguments:
- tokens: bfloat16 [256, 2048], P('grp', ('kv', 'tp')), parts along dimension 0, may hold values from -13 to 13, as said below
- state: float32 [256, 16, 128, 128], P(('grp', 'kv'), 'tp'), parts along dimension 0, may hold values from -0.6 to 0.6
- norm_gain: bfloat16 [2048], P('kv'), may hold values from 0.099609375 to 1.8984375
- w_query: bfloat16 [2048, 2048], P('kv', 'tp'), may hold values from -0.125 to 0.125
- w_key: bfloat16 [2048, 2048], P('kv', 'tp'), may hold values from -0.125 to 0.125
- w_value: bfloat16 [2048, 2048], P('kv', 'tp'), may hold values from -0.125 to 0.125
- w_beta: bfloat16 [2048, 16], replicated, may hold values from -0.125 to 0.125
- w_decay: bfloat16 [2048, 16], replicated, may hold values from -0.125 to 0.125
- a_log: float32 [16], P('tp'), may hold values from -3 to 1
- dt_bias: float32 [16], P('tp'), may hold values from -2 to 1
- head_gain: float32 [128], replicated, may hold values from 0.1 to 1.9
- w_out: bfloat16 [2048, 2048], P('tp', 'kv'), may hold values from -0.125 to 0.125
- mixer_gain: bfloat16 [2048], P('kv'), may hold values from 0.099609375 to 1.8984375
- w_up: bfloat16 [2048, 8192], P('kv', 'tp'), may hold values from -0.125 to 0.125
- w_down: bfloat16 [8192, 2048], P('tp', 'kv'), may hold values from -0.0625 to 0.0625
Outputs:
- mixed: bfloat16 [256, 2048], P('grp', ('kv', 'tp')), parts along dimension 0
- new_state: float32 [256, 16, 128, 128], P(('grp', 'kv'), 'tp'), parts along dimension 0
There are 2 independent parts, one for each index of `grp`. A program takes and returns all parts, laid end to end along the dimension named above; an argument that names none is the same for every part. Nothing has to cross between parts.
Inputs may be any that keep to these rules, and one draw needn't show every extreme that they name: `tokens`: activations of order one.
All inputs are finite; a program needn't handle non-finite values.
Results may differ from a plain program's by a relative error of at most 0.019.
Values may be sent and summed in bfloat16 or wider, within the bound.
No kernel may reach another device: no remote copies, remote signals or barrier semaphores. Data moves between devices by JAX's collectives and lax.ppermute only.
A program may use at most 64 MiB of HBM per device.

v0:
```python
import jax
import jax.numpy as jnp
from jax import lax
from jax.sharding import PartitionSpec as P

D = 2048


epsilon = 1e-06


def joined_along(parts, dim):
    shape = list(parts.shape[1:])
    shape[dim] *= parts.shape[0]
    return jnp.moveaxis(parts, 0, dim).reshape(shape)


def from_everyone(x, axis):
    copies = jnp.broadcast_to(x, (lax.axis_size(axis), *x.shape))
    return lax.all_to_all(copies, axis, split_axis=0, concat_axis=0, tiled=True)


def gather_directly(x, axis, dim):
    return joined_along(from_everyone(x, axis), dim)


def split_up(x, dim, devices):
    before, after = (x.shape[:dim], x.shape[dim + 1 :])
    return jnp.moveaxis(x.reshape(*before, devices, -1, *after), dim, 0)


def sent_and_summed(x, axis, dim):
    parts = split_up(x, dim, lax.axis_size(axis))
    arrived = lax.all_to_all(parts, axis, split_axis=0, concat_axis=0, tiled=True)
    return arrived.sum(axis=0)


def in_one_piece(arrays, axis, dim, along):
    columns = [a.reshape(*a.shape[:along], -1) for a in arrays]
    both = jnp.concatenate(columns, axis=along)
    whole, at, done = (sent_and_summed(both, axis, dim), 0, [])
    for a, column in zip(arrays, columns):
        section = whole[..., at : at + column.shape[along]]
        done.append(section.reshape(*section.shape[:along], *a.shape[along:]))
        at += column.shape[along]
    return tuple(done)


def summed_on_arrival(x, axis, dim):
    parts = split_up(x, dim, lax.axis_size(axis))
    arrived = lax.all_to_all(parts, axis, split_axis=0, concat_axis=0, tiled=True)
    return arrived.astype(jnp.float32).sum(axis=0)


def taken_together(x, axis):
    everything = from_everyone(x, axis)
    return jnp.sum(everything, axis=0)


def dotted(left, right):
    return jnp.dot(left, right, preferred_element_type=jnp.float32)


def delta_update(
    query_pre, key_pre, value_pre, beta_pre, decay_pre, state, a_log, dt_bias, head_gain
):
    query = query_pre * lax.rsqrt(jnp.sum(query_pre * query_pre, axis=-1, keepdims=True) + epsilon)
    keyed = key_pre * lax.rsqrt(jnp.sum(key_pre * key_pre, axis=-1, keepdims=True) + epsilon)
    beta = jax.nn.sigmoid(beta_pre)
    decay = jnp.exp(-jnp.exp(a_log) * jax.nn.softplus(decay_pre + dt_bias))
    key_read = jnp.einsum("bhk,bhkv->bhv", keyed, state)
    query_read = jnp.einsum("bhk,bhkv->bhv", query, state)
    fresh = beta[..., None] * (value_pre - decay[..., None] * key_read)
    new_state = decay[..., None, None] * state + keyed[..., :, None] * fresh[..., None, :]
    intersection = jnp.sum(query * keyed, axis=-1)
    reading = decay[..., None] * query_read + intersection[..., None] * fresh
    normed = (
        reading
        * lax.rsqrt(jnp.mean(reading * reading, axis=-1, keepdims=True) + epsilon)
        * head_gain
    )
    return (normed.astype(jnp.bfloat16), new_state)


def local(
    tokens,
    state,
    norm_gain,
    w_query,
    w_key,
    w_value,
    w_beta,
    w_decay,
    a_log,
    dt_bias,
    head_gain,
    w_out,
    mixer_gain,
    w_up,
    w_down,
):
    seq_here = state.shape[0]
    heads_here = state.shape[1]
    head_size = state.shape[2]
    kv_index = lax.axis_index("kv")
    tp_index = lax.axis_index("tp")
    gathered = gather_directly(tokens, "tp", 1)
    block = gathered.shape[1]
    inputs = gathered.astype(jnp.float32)
    scaled = (inputs * norm_gain.astype(jnp.float32)).astype(jnp.bfloat16)
    partial_sq = jnp.sum(inputs * inputs, axis=1)
    beta_rows = lax.dynamic_slice(
        w_beta, (kv_index * block, tp_index * heads_here), (block, heads_here)
    )
    decay_rows = lax.dynamic_slice(
        w_decay, (kv_index * block, tp_index * heads_here), (block, heads_here)
    )
    query_part = dotted(scaled, w_query)
    key_part = dotted(scaled, w_key)
    value_part = dotted(scaled, w_value)
    beta_part = dotted(scaled, beta_rows)
    decay_part = dotted(scaled, decay_rows)
    query_sum, key_sum, value_sum, beta_sum, decay_sum, square_sum = in_one_piece(
        (query_part, key_part, value_part, beta_part, decay_part, partial_sq), "kv", 0, 1
    )
    first = lax.rsqrt(square_sum / D + epsilon)[:, None]
    query_pre = (first * query_sum).reshape(seq_here, heads_here, head_size)
    key_pre = (first * key_sum).reshape(seq_here, heads_here, head_size)
    value_pre = (first * value_sum).reshape(seq_here, heads_here, head_size)
    normed, new_state = delta_update(
        query_pre,
        key_pre,
        value_pre,
        first * beta_sum,
        first * decay_sum,
        state,
        a_log,
        dt_bias,
        head_gain,
    )
    normed = normed.reshape(seq_here, heads_here * head_size)
    head_part = dotted(gather_directly(normed, "kv", 0), w_out)
    attended = summed_on_arrival(head_part.astype(jnp.bfloat16), "tp", 1)
    middle = (tokens.astype(jnp.float32) + attended).astype(jnp.bfloat16)
    middle_rows = gather_directly(middle, "tp", 1).astype(jnp.float32)
    square_two = taken_together(jnp.sum(middle_rows * middle_rows, axis=1), "kv")
    second = lax.rsqrt(square_two / D + epsilon)[:, None]
    scaled_two = (middle_rows * mixer_gain.astype(jnp.float32)).astype(jnp.bfloat16)
    up_part = dotted(scaled_two, w_up)
    up_share = sent_and_summed(up_part, "kv", 1)
    hidden_share = jnp.square(jax.nn.relu(second * up_share)).astype(jnp.bfloat16)
    down_part = dotted(gather_directly(hidden_share, "kv", 1), w_down)
    lowered = summed_on_arrival(down_part.astype(jnp.bfloat16), "tp", 1)
    mixed = (middle.astype(jnp.float32) + lowered).astype(jnp.bfloat16)
    return (mixed, new_state)


def solution(mesh):
    return jax.shard_map(
        local,
        mesh=mesh,
        in_specs=(
            P("grp", ("kv", "tp")),
            P(("grp", "kv"), "tp", None, None),
            P("kv"),
            P("kv", "tp"),
            P("kv", "tp"),
            P("kv", "tp"),
            P(),
            P(),
            P("tp"),
            P("tp"),
            P(),
            P("tp", "kv"),
            P("kv"),
            P("kv", "tp"),
            P("tp", "kv"),
        ),
        out_specs=(P("grp", ("kv", "tp")), P(("grp", "kv"), "tp", None, None)),
        check_vma=False,
    )
```

profile of v0, /device:TPU:33, one launch (start us, length us, event | category | flops | bytes accessed | tf_op | source)
XLA Modules:
  0.0 324.2 jit_solution(18350188781352569365)
XLA Ops:
  0.6 0.0 copy-start
  0.6 1.3 broadcast_in_dim.10
  2.0 44.7 %all-to-all-start = ((bf16[8,128,8]{1,2,0:T(8,128)(2,1)}), bf16[8,128,8]{1,2,0:T(8,128)(2,1)S(1)}, u32[]{:S(2)}, u32[]{:S(2)}) async-start(bf16[8,128,8]{1,2,0:T(8,128)(2,1)} %broadcast_in_dim.10), calls=%async_computation | async-start | bytes 32768 | tf_op jit(solution)/shard_map/all_to_all | solution.py:20
  46.7 0.7 copy-done.11
  47.3 4.1 %all-to-all-done = bf16[8,128,8]{1,2,0:T(8,128)(2,1)S(1)} async-done(((bf16[8,128,8]{1,2,0:T(8,128)(2,1)}), bf16[8,128,8]{1,2,0:T(8,128)(2,1)S(1)}, u32[]{:S(2)}, u32[]{:S(2)}) %all-to-all-start) | async-done | bytes 16416 | tf_op jit(solution)/shard_map/all_to_all | solution.py:20
  51.4 0.2 copy.142
  51.6 0.2 reshape.133
  51.8 0.7 copy-done.4
  52.6 0.1 fusion.10
  52.7 0.6 copy-done.5
  53.3 0.1 fusion.8
  53.5 0.6 copy-done.6
  54.1 0.1 fusion.6
  54.2 0.9 fusion.32
  55.1 0.9 fusion.30
  56.0 0.1 concatenate.6
  56.1 0.3 copy.146
  56.5 0.1 concatenate.7
  56.6 1.1 copy.147
  57.7 6.9 %all-to-all-start.1 = ((f32[32,4,773]{2,1,0:T(4,128)}), f32[32,4,773]{2,1,0:T(4,128)S(1)}, u32[]{:S(2)}, u32[]{:S(2)}) async-start(f32[32,4,773]{2,1,0:T(4,128)} %copy.147), calls=%async_computation.1 | async-start | bytes 917504 | tf_op jit(solution)/shard_map/all_to_all | solution.py:34
  64.6 57.9 %all-to-all-done.1 = f32[32,4,773]{2,1,0:T(4,128)S(1)} async-done(((f32[32,4,773]{2,1,0:T(4,128)}), f32[32,4,773]{2,1,0:T(4,128)S(1)}, u32[]{:S(2)}, u32[]{:S(2)}) %all-to-all-start.1) | async-done | bytes 395808 | tf_op jit(solution)/shard_map/all_to_all | solution.py:34
  122.5 0.1 reduce_sum.100
  122.5 0.2 fusion.29
  122.7 0.1 slice_multiply_fusion.1
  122.8 0.1 multiply_reduce_fusion.2
  122.9 0.1 multiply_reduce_fusion.3
  123.0 0.2 multiply_reduce_fusion.1
  123.2 0.1 copy.149
  123.3 0.6 copy-done.9
  123.9 0.1 fusion.25
  124.0 0.1 copy.148
  124.1 0.2 fusion.37
  124.2 0.2 fusion.38
  124.4 0.1 copy.150
  124.5 0.2 multiply_reduce_fusion
  124.7 0.1 copy.151
  124.8 0.1 copy.152
  124.9 0.7 copy-done.8
  125.5 0.1 fusion.19
  125.7 26.7 %all_to_all.46 = bf16[32,4,256]{2,1,0:T(4,128)(2,1)S(1)} all-to-all(bf16[32,4,256]{2,1,0:T(4,128)(2,1)S(1)} %broadcast_in_dim.11), channel_id=1, replica_groups=mesh['grp'=2,'kv'=32,'tp'=8] {'kv'}, dimensions={0} | all-to-all | bytes 131072 | tf_op jit(solution)/shard_map/all_to_all | solution.py:20
  152.4 0.7 copy-done.3
  153.1 0.1 fusion
  153.2 10.6 %all_to_all.47 = bf16[8,128,8]{1,2,0:T(8,128)(2,1)S(1)} all-to-all(bf16[8,128,8]{1,2,0:T(8,128)(2,1)S(1)} %fusion), channel_id=1, replica_groups=mesh['grp'=2,'kv'=32,'tp'=8] {'tp'}, dimensions={0} | all-to-all | bytes 32768 | tf_op jit(solution)/shard_map/all_to_all | solution.py:51
  163.8 0.7 copy-done.7
  164.5 0.6 broadcast_in_dim.12
  165.1 4.0 %all-to-all-start.4 = ((bf16[8,128,8]{1,2,0:T(8,128)(2,1)}), bf16[8,128,8]{1,2,0:T(8,128)(2,1)S(1)}, u32[]{:S(2)}, u32[]{:S(2)}) async-start(bf16[8,128,8]{1,2,0:T(8,128)(2,1)} %broadcast_in_dim.12), calls=%async_computation.4 | async-start | bytes 32768 | tf_op jit(solution)/shard_map/all_to_all | solution.py:20
  169.1 0.2 copy.154
  169.2 0.5 copy-done.10
  169.7 0.1 reshape.134
  169.8 4.0 %all-to-all-done.4 = bf16[8,128,8]{1,2,0:T(8,128)(2,1)S(1)} async-done(((bf16[8,128,8]{1,2,0:T(8,128)(2,1)}), bf16[8,128,8]{1,2,0:T(8,128)(2,1)S(1)}, u32[]{:S(2)}, u32[]{:S(2)}) %all-to-all-start.4) | async-done | bytes 16416 | tf_op jit(solution)/shard_map/all_to_all | solution.py:20
  173.8 0.6 broadcast_in_dim.13
  174.4 4.8 %all-to-all-start.5 = ((f32[32,1,128]{2,1,0:T(1,128)}), f32[32,1,128]{2,1,0:T(1,128)S(1)}, u32[]{:S(2)}, u32[]{:S(2)}) async-start(f32[32,1,128]{2,1,0:T(1,128)} %broadcast_in_dim.13), calls=%async_computation.5 | async-start | bytes 32768 | tf_op jit(solution)/shard_map/all_to_all | solution.py:20
  179.2 1.1 convolution_bitcast_fusion
  180.3 19.3 %all-to-all-done.5 = f32[32,1,128]{2,1,0:T(1,128)S(1)} async-done(((f32[32,1,128]{2,1,0:T(1,128)}), f32[32,1,128]{2,1,0:T(1,128)S(1)}, u32[]{:S(2)}, u32[]{:S(2)}) %all-to-all-start.5) | async-done | bytes 16416 | tf_op jit(solution)/shard_map/all_to_all | solution.py:20
  199.6 4.8 %all-to-all-start.6 = ((f32[32,128,32]{1,2,0:T(8,128)}), f32[32,128,32]{1,2,0:T(8,128)S(1)}, u32[]{:S(2)}, u32[]{:S(2)}) async-start(f32[32,128,32]{1,2,0:T(8,128)} %convolution_bitcast_fusion), calls=%async_computation.6 | async-start | bytes 1048576 | tf_op jit(solution)/shard_map/all_to_all | solution.py:34
  204.4 60.8 %all-to-all-done.6 = f32[32,128,32]{1,2,0:T(8,128)S(1)} async-done(((f32[32,128,32]{1,2,0:T(8,128)}), f32[32,128,32]{1,2,0:T(8,128)S(1)}, u32[]{:S(2)}, u32[]{:S(2)}) %all-to-all-start.6) | async-done | bytes 524320 | tf_op jit(solution)/shard_map/all_to_all | solution.py:34
  265.3 0.7 broadcast_in_dim.14
  266.0 6.1 %all-to-all-start.7 = ((bf16[32,128,32]{1,2,0:T(8,128)(2,1)}), bf16[32,128,32]{1,2,0:T(8,128)(2,1)S(1)}, u32[]{:S(2)}, u32[]{:S(2)}) async-start(bf16[32,128,32]{1,2,0:T(8,128)(2,1)} %broadcast_in_dim.14), calls=%async_computation.7 | async-start | bytes 524288 | tf_op jit(solution)/shard_map/all_to_all | solution.py:20
  272.1 37.3 %all-to-all-done.7 = bf16[32,128,32]{1,2,0:T(8,128)(2,1)S(1)} async-done(((bf16[32,128,32]{1,2,0:T(8,128)(2,1)}), bf16[32,128,32]{1,2,0:T(8,128)(2,1)S(1)}, u32[]{:S(2)}, u32[]{:S(2)}) %all-to-all-start.7) | async-done | bytes 262176 | tf_op jit(solution)/shard_map/all_to_all | solution.py:20
  309.5 0.8 fusion.1
  310.2 8.7 %all-to-all-start.8 = ((bf16[8,128,8]{1,2,0:T(8,128)(2,1)}), bf16[8,128,8]{1,2,0:T(8,128)(2,1)S(1)}, u32[]{:S(2)}, u32[]{:S(2)}) async-start(bf16[8,128,8]{1,2,0:T(8,128)(2,1)} %fusion.1), calls=%async_computation.8 | async-start | bytes 32768 | tf_op jit(solution)/shard_map/all_to_all | solution.py:51
  318.9 1.0 multiply_add_fusion
  319.9 3.7 %all-to-all-done.8 = bf16[8,128,8]{1,2,0:T(8,128)(2,1)S(1)} async-done(((bf16[8,128,8]{1,2,0:T(8,128)(2,1)}), bf16[8,128,8]{1,2,0:T(8,128)(2,1)S(1)}, u32[]{:S(2)}, u32[]{:S(2)}) %all-to-all-start.8) | async-done | bytes 16416 | tf_op jit(solution)/shard_map/all_to_all | solution.py:51
  323.6 0.6 add_convert_fusion
  (36 shorter events, 0.3 us)
Async XLA Ops:
  0.6 308.8 %copy-start = (bf16[1024,64]{0,1:T(8,128)(2,1)S(1)}, bf16[1024,64]{0,1:T(8,128)(2,1)}, u32[]{:S(2)}) copy-start(bf16[1024,64]{0,1:T(8,128)(2,1)} %param.29) | copy-start | bytes 393220
  2.0 49.4 %all-to-all-start = ((bf16[8,128,8]{1,2,0:T(8,128)(2,1)}), bf16[8,128,8]{1,2,0:T(8,128)(2,1)S(1)}, u32[]{:S(2)}, u32[]{:S(2)}) async-start(bf16[8,128,8]{1,2,0:T(8,128)(2,1)} %broadcast_in_dim.10), calls=%async_computation | async-start | bytes 32768 | tf_op jit(solution)/shard_map/all_to_all | solution.py:20
  46.7 0.7 copy-start.11
  51.8 0.8 copy-start.4
  52.6 0.8 copy-start.5
  53.3 0.8 copy-start.6
  57.6 6.9 %copy-start.12 = (f32[2]{0:T(128)S(1)}, f32[2]{0:T(128)}, u32[]{:S(2)}) copy-start(f32[2]{0:T(128)} %param.23) | copy-start | bytes 28
  57.7 66.4 %copy-start.1 = (f32[4,2,128,128]{3,2,1,0:T(8,128)S(1)}, f32[4,2,128,128]{3,2,1,0:T(8,128)}, u32[]{:S(2)}) copy-start(f32[4,2,128,128]{3,2,1,0:T(8,128)} %param.16) | copy-start | bytes 1572868
  57.7 64.8 %all-to-all-start.1 = ((f32[32,4,773]{2,1,0:T(4,128)}), f32[32,4,773]{2,1,0:T(4,128)S(1)}, u32[]{:S(2)}, u32[]{:S(2)}) async-start(f32[32,4,773]{2,1,0:T(4,128)} %copy.147), calls=%async_computation.1 | async-start | bytes 917504 | tf_op jit(solution)/shard_map/all_to_all | solution.py:34
  123.2 0.7 copy-start.9
  124.9 0.7 copy-start.8
  152.4 0.8 copy-start.3
  153.1 15.9 %copy-start.2 = (bf16[64,1024]{1,0:T(8,128)(2,1)S(1)}, bf16[64,1024]{1,0:T(8,128)(2,1)}, u32[]{:S(2)}) copy-start(bf16[64,1024]{1,0:T(8,128)(2,1)} %param.28) | copy-start | bytes 393220
  163.8 0.7 copy-start.7
  165.1 8.7 %all-to-all-start.4 = ((bf16[8,128,8]{1,2,0:T(8,128)(2,1)}), bf16[8,128,8]{1,2,0:T(8,128)(2,1)S(1)}, u32[]{:S(2)}, u32[]{:S(2)}) async-start(bf16[8,128,8]{1,2,0:T(8,128)(2,1)} %broadcast_in_dim.12), calls=%async_computation.4 | async-start | bytes 32768 | tf_op jit(solution)/shard_map/all_to_all | solution.py:20
  169.1 0.7 copy-start.10
  174.4 25.2 %all-to-all-start.5 = ((f32[32,1,128]{2,1,0:T(1,128)}), f32[32,1,128]{2,1,0:T(1,128)S(1)}, u32[]{:S(2)}, u32[]{:S(2)}) async-start(f32[32,1,128]{2,1,0:T(1,128)} %broadcast_in_dim.13), calls=%async_computation.5 | async-start | bytes 32768 | tf_op jit(solution)/shard_map/all_to_all | solution.py:20
  199.6 65.6 %all-to-all-start.6 = ((f32[32,128,32]{1,2,0:T(8,128)}), f32[32,128,32]{1,2,0:T(8,128)S(1)}, u32[]{:S(2)}, u32[]{:S(2)}) async-start(f32[32,128,32]{1,2,0:T(8,128)} %convolution_bitcast_fusion), calls=%async_computation.6 | async-start | bytes 1048576 | tf_op jit(solution)/shard_map/all_to_all | solution.py:34
  266.0 43.4 %all-to-all-start.7 = ((bf16[32,128,32]{1,2,0:T(8,128)(2,1)}), bf16[32,128,32]{1,2,0:T(8,128)(2,1)S(1)}, u32[]{:S(2)}, u32[]{:S(2)}) async-start(bf16[32,128,32]{1,2,0:T(8,128)(2,1)} %broadcast_in_dim.14), calls=%async_computation.7 | async-start | bytes 524288 | tf_op jit(solution)/shard_map/all_to_all | solution.py:20
  310.2 13.4 %all-to-all-start.8 = ((bf16[8,128,8]{1,2,0:T(8,128)(2,1)}), bf16[8,128,8]{1,2,0:T(8,128)(2,1)S(1)}, u32[]{:S(2)}, u32[]{:S(2)}) async-start(bf16[8,128,8]{1,2,0:T(8,128)(2,1)} %fusion.1), calls=%async_computation.8 | async-start | bytes 32768 | tf_op jit(solution)/shard_map/all_to_all | solution.py:51
where the time goes:
time: 325 us; the launch traced here: 324 us
  waiting for transfers between devices  187 us (58%)
  starting transfers between devices  79.9 us (25%)
  blocking collectives  37.3 us (11%)
  local copies, waits for them, and re-layouts  11.9 us (4%)
  matrix products  4.48 us (1%)
    all_to_all x2, waiting for transfers between devices, sent_and_summed(): lax.all_to_all(parts, axis, split_axis=0, concat_axis=0, tiled=True)  119 us
    all_to_all x4, waiting for transfers between devices, from_everyone(): return lax.all_to_all(copies, axis, split_axis=0, concat_axis=0, tiled=True)  64.7 us
    all_to_all x4, starting transfers between devices, from_everyone(): return lax.all_to_all(copies, axis, split_axis=0, concat_axis=0, tiled=True)  59.5 us
    all_to_all x1, blocking collectives, from_everyone(): return lax.all_to_all(copies, axis, split_axis=0, concat_axis=0, tiled=True)  26.7 us
    all_to_all x2, starting transfers between devices, sent_and_summed(): lax.all_to_all(parts, axis, split_axis=0, concat_axis=0, tiled=True)  11.7 us
    all_to_all x1, blocking collectives, summed_on_arrival(): lax.all_to_all(parts, axis, split_axis=0, concat_axis=0, tiled=True)  10.6 us
    all_to_all x1, starting transfers between devices, summed_on_arrival(): lax.all_to_all(parts, axis, split_axis=0, concat_axis=0, tiled=True)  8.68 us
  transfers between devices with their start and end apart: 7, of which 7 were waited for; matrix products, arithmetic and copies ran while one was open for 1% of the time, Pallas kernels for 0%

commit v1 on v0

v1 whole, which is shorter than its diff:
```python
import jax
import jax.numpy as jnp
from jax import lax
from jax.sharding import PartitionSpec as P

epsilon = 1e-06
bf16 = jnp.bfloat16
f32 = jnp.float32


def exchange(x, axis):
    return lax.all_to_all(x, axis, split_axis=0, concat_axis=0, tiled=True)


def from_everyone(x, axis):
    return exchange(jnp.broadcast_to(x, (lax.axis_size(axis), *x.shape)), axis)


def dotted(left, right, left_dim, right_dim):
    dims = (((left_dim,), (right_dim,)), ((), ()))
    return lax.dot_general(left, right, dims, preferred_element_type=f32)


def delta_update(
    query_pre, key_pre, value_pre, beta_pre, decay_pre, state, a_log, dt_bias, head_gain
):
    query = query_pre * lax.rsqrt(jnp.sum(query_pre * query_pre, axis=-1, keepdims=True) + epsilon)
    keyed = key_pre * lax.rsqrt(jnp.sum(key_pre * key_pre, axis=-1, keepdims=True) + epsilon)
    beta = jax.nn.sigmoid(beta_pre)
    decay = jnp.exp(-jnp.exp(a_log) * jax.nn.softplus(decay_pre + dt_bias))
    key_read = jnp.einsum("bhk,bhkv->bhv", keyed, state)
    query_read = jnp.einsum("bhk,bhkv->bhv", query, state)
    fresh = beta[..., None] * (value_pre - decay[..., None] * key_read)
    new_state = decay[..., None, None] * state + keyed[..., :, None] * fresh[..., None, :]
    intersection = jnp.sum(query * keyed, axis=-1)
    reading = decay[..., None] * query_read + intersection[..., None] * fresh
    normed = (
        reading
        * lax.rsqrt(jnp.mean(reading * reading, axis=-1, keepdims=True) + epsilon)
        * head_gain
    )
    return (normed.astype(bf16), new_state)


def mixer_weights(w_up, w_down, mixer_gain, n_kv, n_tp):
    gained = (w_up.astype(f32) * mixer_gain.astype(f32)[:, None]).astype(bf16)
    own = gained.shape[0] // n_tp
    wide = gained.shape[1]
    both = jnp.stack([gained.reshape(n_tp, own, wide), w_down.T.reshape(n_tp, own, wide)], axis=1)
    arrived = exchange(both, "tp")
    hidden_here = wide * n_tp // n_kv
    pieces = arrived.reshape(n_tp, 2, own, wide // hidden_here, hidden_here)
    pieces = pieces.transpose(0, 3, 1, 2, 4).reshape(n_kv, 2, own, hidden_here)
    whole = exchange(pieces, "kv")
    up = whole[:, 0].reshape(n_kv * own, hidden_here)
    down_t = whole[:, 1].reshape(n_kv * own, hidden_here)
    return up, down_t


def local(
    tokens,
    state,
    norm_gain,
    w_query,
    w_key,
    w_value,
    w_beta,
    w_decay,
    a_log,
    dt_bias,
    head_gain,
    w_out,
    mixer_gain,
    w_up,
    w_down,
):
    seq_here, heads_here, head_size = state.shape[:3]
    n_kv = lax.axis_size("kv")
    n_tp = lax.axis_size("tp")
    width = w_beta.shape[0]
    rows, own = tokens.shape
    block = own * n_tp
    kv_index = lax.axis_index("kv")
    tp_index = lax.axis_index("tp")
    columns = heads_here * head_size

    tokens_t = tokens.T
    inputs = from_everyone(tokens_t, "tp").reshape(block, rows).astype(f32)
    scaled = (inputs * norm_gain.astype(f32)[:, None]).astype(bf16)
    squares = jnp.sum(inputs * inputs, axis=0)
    at = (kv_index * block, tp_index * heads_here)
    beta_rows = lax.dynamic_slice(w_beta, at, (block, heads_here))
    decay_rows = lax.dynamic_slice(w_decay, at, (block, heads_here))
    parts = [
        dotted(scaled, w_query, 0, 0).astype(bf16),
        dotted(scaled, w_key, 0, 0).astype(bf16),
        dotted(scaled, w_value, 0, 0).astype(bf16),
        dotted(scaled, jnp.concatenate([beta_rows, decay_rows], axis=1), 0, 0).astype(bf16),
        squares[:, None].astype(bf16),
    ]
    sent = jnp.concatenate(parts, axis=1).reshape(n_kv, seq_here, -1)
    sums = exchange(sent, "kv").astype(f32).sum(axis=0)
    first = lax.rsqrt(sums[:, -1:] / width + epsilon)
    pre = first * sums
    heads = lambda n: pre[:, n * columns : (n + 1) * columns].reshape(seq_here, heads_here, head_size)
    gates = pre[:, 3 * columns :]
    normed, new_state = delta_update(
        heads(0),
        heads(1),
        heads(2),
        gates[:, :heads_here],
        gates[:, heads_here : 2 * heads_here],
        state,
        a_log,
        dt_bias,
        head_gain,
    )
    up, down_t = mixer_weights(w_up, w_down, mixer_gain, n_kv, n_tp)

    every = from_everyone(normed.reshape(seq_here, columns), "kv").reshape(rows, columns)
    head_part = dotted(w_out, every, 0, 1).astype(bf16)
    arrived = exchange(head_part.reshape(n_tp, own, rows), "tp")
    middle_own = (tokens_t.astype(f32) + arrived.astype(f32).sum(axis=0)).astype(bf16)

    middle = from_everyone(middle_own, "kv").reshape(n_kv * own, rows)
    middle_f = middle.astype(f32)
    squares_two = jnp.sum(middle_f * middle_f, axis=0, keepdims=True)
    hidden_part = dotted(up, middle, 0, 0)
    tail = jnp.broadcast_to(squares_two, (8, rows))
    sent = jnp.concatenate([hidden_part, tail], axis=0).astype(bf16)
    sums = from_everyone(sent, "tp").astype(f32).sum(axis=0)
    second = lax.rsqrt(sums[-1:] / width + epsilon)
    hidden = jnp.square(jax.nn.relu(second * sums[:-8])).astype(bf16)
    down_part = dotted(down_t, hidden, 1, 0).astype(bf16)
    lowered = exchange(down_part.reshape(n_kv, own, rows), "kv").astype(f32).sum(axis=0)
    mixed = (middle_own.astype(f32) + lowered).astype(bf16).T
    return (mixed, new_state)


def solution(mesh):
    return jax.shard_map(
        local,
        mesh=mesh,
        in_specs=(
            P("grp", ("kv", "tp")),
            P(("grp", "kv"), "tp", None, None),
            P("kv"),
            P("kv", "tp"),
            P("kv", "tp"),
            P("kv", "tp"),
            P(),
            P(),
            P("tp"),
            P("tp"),
            P(),
            P("tp", "kv"),
            P("kv"),
            P("kv", "tp"),
            P("tp", "kv"),
        ),
        out_specs=(P("grp", ("kv", "tp")), P(("grp", "kv"), "tp", None, None)),
        check_vma=False,
    )
```

time: 325 us -> 273 us (0.84)
  waiting for transfers between devices: 187 us -> 155 us
  blocking collectives: 37.3 us -> 18.5 us
  local copies, waits for them, and re-layouts: 11.9 us -> 6.15 us
    all_to_all x7 -> x8, waiting for transfers between devices: 187 us -> 155 us  [exchange(): return lax.all_to_all(x, axis, split_axis=0, concat_axis=0, tiled=True)]
    all_to_all x2 -> x1, blocking collectives: 37.3 us -> 18.5 us  [exchange(): return lax.all_to_all(x, axis, split_axis=0, concat_axis=0, tiled=True)]
    unnamed x27 -> x22, local copies, waits for them, and re-layouts: 5.95 us -> 0.05 us
    all_to_all x7 -> x8, starting transfers between devices: 79.9 us -> 81.7 us  [exchange(): return lax.all_to_all(x, axis, split_axis=0, concat_axis=0, tiled=True)]
  transfers between devices with their start and end apart: 7 -> 8, of which waited for: 7 -> 8; matrix products, arithmetic and copies ran while one was open for 1% -> 2% of each run, Pallas kernels for 0% -> 0%
where the time goes in v1:
time: 273 us; the launch traced here: 272 us
  waiting for transfers between devices  155 us (57%)
  starting transfers between devices  81.7 us (30%)
  blocking collectives  18.5 us (7%)
  local copies, waits for them, and re-layouts  6.15 us (2%)
  other arithmetic  5.09 us (2%)
  matrix products  3.88 us (1%)
    all_to_all x8, waiting for transfers between devices, exchange(): return lax.all_to_all(x, axis, split_axis=0, concat_axis=0, tiled=True)  155 us
    all_to_all x8, starting transfers between devices, exchange(): return lax.all_to_all(x, axis, split_axis=0, concat_axis=0, tiled=True)  81.7 us
    all_to_all x1, blocking collectives, exchange(): return lax.all_to_all(x, axis, split_axis=0, concat_axis=0, tiled=True)  18.5 us
  transfers between devices with their start and end apart: 8, of which 8 were waited for; matrix products, arithmetic and copies ran while one was open for 2% of the time, Pallas kernels for 0%

profile of v1, /device:TPU:33, one launch (start us, length us, event | category | flops | bytes accessed | tf_op | source)
XLA Modules:
  0.0 271.5 jit_solution(17983403895631086983)
XLA Ops:
  0.6 0.0 copy-start
  0.7 1.3 broadcast_in_dim.10
  2.0 44.7 %all-to-all-start = ((bf16[8,8,128]{2,1,0:T(8,128)(2,1)}), bf16[8,8,128]{2,1,0:T(8,128)(2,1)S(1)}, u32[]{:S(2)}, u32[]{:S(2)}) async-start(bf16[8,8,128]{2,1,0:T(8,128)(2,1)} %broadcast_in_dim.10), calls=%async_computation | async-start | bytes 32768 | tf_op jit(solution)/shard_map/all_to_all | solution.py:12
  46.6 0.7 convert_element_type.106
  47.3 0.8 dynamic_slice.6
  48.1 0.8 dynamic_slice.7
  48.8 2.5 all-to-all-done
  51.3 0.2 convolution_convert_fusion.6
  51.5 0.1 copy.74
  51.7 0.2 convert_element_type.134
  52.0 0.3 convolution_convert_fusion.1
  52.3 1.0 convolution_convert_fusion
  53.3 0.0 copy-done.4
  53.3 0.3 convolution_convert_fusion.2
  53.6 0.0 copy-start.9
  53.6 0.0 copy-start.8
  53.6 0.9 concatenate.27
  54.6 6.9 %all-to-all-start.1 = ((bf16[32,4,773]{2,1,0:T(4,128)(2,1)}), bf16[32,4,773]{2,1,0:T(4,128)(2,1)S(1)}, u32[]{:S(2)}, u32[]{:S(2)}) async-start(bf16[32,4,773]{2,1,0:T(4,128)(2,1)} %concatenate.27), calls=%async_computation.1 | async-start | bytes 458752 | tf_op jit(solution)/shard_map/all_to_all | solution.py:12
  61.5 0.0 copy-done.9
  61.5 37.3 %all-to-all-done.1 = bf16[32,4,773]{2,1,0:T(4,128)(2,1)S(1)} async-done(((bf16[32,4,773]{2,1,0:T(4,128)(2,1)}), bf16[32,4,773]{2,1,0:T(4,128)(2,1)S(1)}, u32[]{:S(2)}, u32[]{:S(2)}) %all-to-all-start.1) | async-done | bytes 197920 | tf_op jit(solution)/shard_map/all_to_all | solution.py:12
  98.8 0.1 convert_reduce_fusion.1
  98.9 0.2 fusion.26
  99.1 0.1 broadcast_multiply_fusion
  99.2 0.1 fusion.23
  99.3 0.1 copy.66
  99.4 0.1 copy.64
  99.5 0.1 multiply_reduce_fusion.3
  99.6 0.1 multiply_reduce_fusion.4
  99.7 0.2 multiply_reduce_fusion.2
  99.9 0.1 copy.65
  100.0 0.0 copy-start.2
  100.0 0.2 fusion.42
  100.2 0.2 fusion.43
  100.4 0.2 multiply_reduce_fusion.1
  100.5 0.1 copy.67
  100.6 0.1 copy.68
  100.7 0.1 fusion.18
  100.8 0.7 broadcast_in_dim.11
  101.5 4.8 %all-to-all-start.2 = ((bf16[32,4,256]{2,1,0:T(4,128)(2,1)}), bf16[32,4,256]{2,1,0:T(4,128)(2,1)S(1)}, u32[]{:S(2)}, u32[]{:S(2)}) async-start(bf16[32,4,256]{2,1,0:T(4,128)(2,1)} %broadcast_in_dim.11), calls=%async_computation.2 | async-start | bytes 131072 | tf_op jit(solution)/shard_map/all_to_all | solution.py:12
  106.2 0.0 copy-done.10
  106.3 0.1 fusion.2
  106.4 22.5 %all-to-all-done.2 = bf16[32,4,256]{2,1,0:T(4,128)(2,1)S(1)} async-done(((bf16[32,4,256]{2,1,0:T(4,128)(2,1)}), bf16[32,4,256]{2,1,0:T(4,128)(2,1)S(1)}, u32[]{:S(2)}, u32[]{:S(2)}) %all-to-all-start.2) | async-done | bytes 65568 | tf_op jit(solution)/shard_map/all_to_all | solution.py:12
  128.9 0.8 fusion.1
  129.6 7.0 %all-to-all-start.3 = ((bf16[8,8,128]{2,1,0:T(8,128)(2,1)}), bf16[8,8,128]{2,1,0:T(8,128)(2,1)S(1)}, u32[]{:S(2)}, u32[]{:S(2)}) async-start(bf16[8,8,128]{2,1,0:T(8,128)(2,1)} %fusion.1), calls=%async_computation.3 | async-start | bytes 32768 | tf_op jit(solution)/shard_map/all_to_all | solution.py:12
  136.6 0.7 pad_maximum_fusion
  137.4 4.0 %all-to-all-done.3 = bf16[8,8,128]{2,1,0:T(8,128)(2,1)S(1)} async-done(((bf16[8,8,128]{2,1,0:T(8,128)(2,1)}), bf16[8,8,128]{2,1,0:T(8,128)(2,1)S(1)}, u32[]{:S(2)}, u32[]{:S(2)}) %all-to-all-start.3) | async-done | bytes 16416 | tf_op jit(solution)/shard_map/all_to_all | solution.py:12
  141.3 4.0 %all-to-all-start.4 = ((bf16[8,2,8,1024]{3,2,1,0:T(8,128)(2,1)}), bf16[8,2,8,1024]{3,2,1,0:T(8,128)(2,1)S(1)}, u32[]{:S(2)}, u32[]{:S(2)}) async-start(bf16[8,2,8,1024]{3,2,1,0:T(8,128)(2,1)} %pad_maximum_fusion), calls=%async_computation.4 | async-start | bytes 524288 | tf_op jit(solution)/shard_map/all_to_all | solution.py:12
  145.4 6.5 %all-to-all-done.4 = bf16[8,2,8,1024]{3,2,1,0:T(8,128)(2,1)S(1)} async-done(((bf16[8,2,8,1024]{3,2,1,0:T(8,128)(2,1)}), bf16[8,2,8,1024]{3,2,1,0:T(8,128)(2,1)S(1)}, u32[]{:S(2)}, u32[]{:S(2)}) %all-to-all-start.4) | async-done | bytes 262176 | tf_op jit(solution)/shard_map/all_to_all | solution.py:12
  151.9 0.6 broadcast_in_dim.12
  152.6 4.8 %all-to-all-start.6 = ((bf16[32,8,128]{2,1,0:T(8,128)(2,1)}), bf16[32,8,128]{2,1,0:T(8,128)(2,1)S(1)}, u32[]{:S(2)}, u32[]{:S(2)}) async-start(bf16[32,8,128]{2,1,0:T(8,128)(2,1)} %broadcast_in_dim.12), calls=%async_computation.6 | async-start | bytes 131072 | tf_op jit(solution)/shard_map/all_to_all | solution.py:12
  157.3 0.7 pad_maximum_fusion.1
  158.1 22.6 %all-to-all-done.6 = bf16[32,8,128]{2,1,0:T(8,128)(2,1)S(1)} async-done(((bf16[32,8,128]{2,1,0:T(8,128)(2,1)}), bf16[32,8,128]{2,1,0:T(8,128)(2,1)S(1)}, u32[]{:S(2)}, u32[]{:S(2)}) %all-to-all-start.6) | async-done | bytes 65568 | tf_op jit(solution)/shard_map/all_to_all | solution.py:12
  180.6 4.8 %all-to-all-start.5 = ((bf16[32,2,8,256]{3,2,1,0:T(8,128)(2,1)}), bf16[32,2,8,256]{3,2,1,0:T(8,128)(2,1)S(1)}, u32[]{:S(2)}, u32[]{:S(2)}) async-start(bf16[32,2,8,256]{3,2,1,0:T(8,128)(2,1)} %bitcast.17), calls=%async_computation.5 | async-start | bytes 524288 | tf_op jit(solution)/shard_map/all_to_all | solution.py:12
  185.4 0.1 multiply_reduce_fusion
  185.5 36.8 %all-to-all-done.5 = bf16[32,2,8,256]{3,2,1,0:T(8,128)(2,1)S(1)} async-done(((bf16[32,2,8,256]{3,2,1,0:T(8,128)(2,1)}), bf16[32,2,8,256]{3,2,1,0:T(8,128)(2,1)S(1)}, u32[]{:S(2)}, u32[]{:S(2)}) %all-to-all-start.5) | async-done | bytes 262176 | tf_op jit(solution)/shard_map/all_to_all | solution.py:12
  222.3 0.2 convolution_convert_fusion.4
  222.5 0.1 broadcast_in_dim.14
  222.6 18.5 %all_to_all.45 = bf16[8,264,128]{2,1,0:T(8,128)(2,1)S(1)} all-to-all(bf16[8,264,128]{2,1,0:T(8,128)(2,1)S(1)} %broadcast_in_dim.14), channel_id=1, replica_groups=mesh['grp'=2,'kv'=32,'tp'=8] {'tp'}, dimensions={0} | all-to-all | bytes 1081344 | tf_op jit(solution)/shard_map/all_to_all | solution.py:12
  241.1 0.1 convert_reduce_fusion
  241.2 0.8 fusion
  242.0 4.8 %all-to-all-start.8 = ((bf16[32,8,128]{2,1,0:T(8,128)(2,1)}), bf16[32,8,128]{2,1,0:T(8,128)(2,1)S(1)}, u32[]{:S(2)}, u32[]{:S(2)}) async-start(bf16[32,8,128]{2,1,0:T(8,128)(2,1)} %fusion), calls=%async_computation.8 | async-start | bytes 131072 | tf_op jit(solution)/shard_map/all_to_all | solution.py:12
  246.8 1.0 multiply_add_fusion
  247.8 23.1 %all-to-all-done.8 = bf16[32,8,128]{2,1,0:T(8,128)(2,1)S(1)} async-done(((bf16[32,8,128]{2,1,0:T(8,128)(2,1)}), bf16[32,8,128]{2,1,0:T(8,128)(2,1)S(1)}, u32[]{:S(2)}, u32[]{:S(2)}) %all-to-all-start.8) | async-done | bytes 65568 | tf_op jit(solution)/shard_map/all_to_all | solution.py:12
  270.9 0.6 fusion.15
  (35 shorter events, 0.3 us)
Async XLA Ops:
  0.6 51.3 %copy-start = (bf16[64,256]{1,0:T(8,128)(2,1)S(1)}, bf16[64,256]{1,0:T(8,128)(2,1)}, u32[]{:S(2)}) copy-start(bf16[64,256]{1,0:T(8,128)(2,1)} %param.19) | copy-start | bytes 98308
  0.6 52.7 %copy-start.4 = (bf16[64,256]{1,0:T(8,128)(2,1)S(1)}, bf16[64,256]{1,0:T(8,128)(2,1)}, u32[]{:S(2)}) copy-start(bf16[64,256]{1,0:T(8,128)(2,1)} %param.18) | copy-start | bytes 98308
  2.0 49.4 %all-to-all-start = ((bf16[8,8,128]{2,1,0:T(8,128)(2,1)}), bf16[8,8,128]{2,1,0:T(8,128)(2,1)S(1)}, u32[]{:S(2)}, u32[]{:S(2)}) async-start(bf16[8,8,128]{2,1,0:T(8,128)(2,1)} %broadcast_in_dim.10), calls=%async_computation | async-start | bytes 32768 | tf_op jit(solution)/shard_map/all_to_all | solution.py:12
  53.6 7.9 %copy-start.9 = (f32[2]{0:T(128)S(1)}, f32[2]{0:T(128)}, u32[]{:S(2)}) copy-start(f32[2]{0:T(128)} %param.23) | copy-start | bytes 28
  53.6 45.6 %copy-start.8 = (f32[2]{0:T(128)S(1)}, f32[2]{0:T(128)}, u32[]{:S(2)}) copy-start(f32[2]{0:T(128)} %param.24) | copy-start | bytes 28
  54.6 45.4 %copy-start.1 = (f32[4,2,128,128]{3,2,1,0:T(8,128)S(1)}, f32[4,2,128,128]{3,2,1,0:T(8,128)}, u32[]{:S(2)}) copy-start(f32[4,2,128,128]{3,2,1,0:T(8,128)} %param.16) | copy-start | bytes 1572868
  54.6 44.2 %all-to-all-start.1 = ((bf16[32,4,773]{2,1,0:T(4,128)(2,1)}), bf16[32,4,773]{2,1,0:T(4,128)(2,1)S(1)}, u32[]{:S(2)}, u32[]{:S(2)}) async-start(bf16[32,4,773]{2,1,0:T(4,128)(2,1)} %concatenate.27), calls=%async_computation.1 | async-start | bytes 458752 | tf_op jit(solution)/shard_map/all_to_all | solution.py:12
  100.0 0.8 copy-start.7
  100.0 6.3 %copy-start.10 = (bf16[64]{0:T(256)(128)(2,1)S(1)}, bf16[64]{0:T(256)(128)(2,1)}, u32[]{:S(2)}) copy-start(bf16[64]{0:T(256)(128)(2,1)} %param.27) | copy-start | bytes 388
  100.0 6.3 %copy-start.2 = (bf16[64,1024]{1,0:T(8,128)(2,1)S(1)}, bf16[64,1024]{1,0:T(8,128)(2,1)}, u32[]{:S(2)}) copy-start(bf16[64,1024]{1,0:T(8,128)(2,1)} %param.28) | copy-start | bytes 393220
  100.2 28.7 %copy-start.5 = (bf16[256,64]{0,1:T(8,128)(2,1)S(1)}, bf16[256,64]{0,1:T(8,128)(2,1)}, u32[]{:S(2)}) copy-start(bf16[256,64]{0,1:T(8,128)(2,1)} %param.26) | copy-start | bytes 98308
  100.2 36.5 %copy-start.3 = (bf16[1024,64]{0,1:T(8,128)(2,1)S(1)}, bf16[1024,64]{0,1:T(8,128)(2,1)}, u32[]{:S(2)}) copy-start(bf16[1024,64]{0,1:T(8,128)(2,1)} %param.29) | copy-start | bytes 393220
  101.5 27.4 %all-to-all-start.2 = ((bf16[32,4,256]{2,1,0:T(4,128)(2,1)}), bf16[32,4,256]{2,1,0:T(4,128)(2,1)S(1)}, u32[]{:S(2)}, u32[]{:S(2)}) async-start(bf16[32,4,256]{2,1,0:T(4,128)(2,1)} %broadcast_in_dim.11), calls=%async_computation.2 | async-start | bytes 131072 | tf_op jit(solution)/shard_map/all_to_all | solution.py:12
  129.6 11.7 %all-to-all-start.3 = ((bf16[8,8,128]{2,1,0:T(8,128)(2,1)}), bf16[8,8,128]{2,1,0:T(8,128)(2,1)S(1)}, u32[]{:S(2)}, u32[]{:S(2)}) async-start(bf16[8,8,128]{2,1,0:T(8,128)(2,1)} %fusion.1), calls=%async_computation.3 | async-start | bytes 32768 | tf_op jit(solution)/shard_map/all_to_all | solution.py:12
  136.6 8.8 %copy-start.6 = (bf16[128,8]{0,1:T(8,128)(2,1)S(1)}, bf16[128,8]{0,1:T(8,128)(2,1)}, u32[]{:S(2)}) copy-start(bf16[128,8]{0,1:T(8,128)(2,1)} %param.15) | copy-start | bytes 6148
  141.3 10.6 %all-to-all-start.4 = ((bf16[8,2,8,1024]{3,2,1,0:T(8,128)(2,1)}), bf16[8,2,8,1024]{3,2,1,0:T(8,128)(2,1)S(1)}, u32[]{:S(2)}, u32[]{:S(2)}) async-start(bf16[8,2,8,1024]{3,2,1,0:T(8,128)(2,1)} %pad_maximum_fusion), calls=%async_computation.4 | async-start | bytes 524288 | tf_op jit(solution)/shard_map/all_to_all | solution.py:12
  152.6 28.1 %all-to-all-start.6 = ((bf16[32,8,128]{2,1,0:T(8,128)(2,1)}), bf16[32,8,128]{2,1,0:T(8,128)(2,1)S(1)}, u32[]{:S(2)}, u32[]{:S(2)}) async-start(bf16[32,8,128]{2,1,0:T(8,128)(2,1)} %broadcast_in_dim.12), calls=%async_computation.6 | async-start | bytes 131072 | tf_op jit(solution)/shard_map/all_to_all | solution.py:12
  180.6 41.6 %all-to-all-start.5 = ((bf16[32,2,8,256]{3,2,1,0:T(8,128)(2,1)}), bf16[32,2,8,256]{3,2,1,0:T(8,128)(2,1)S(1)}, u32[]{:S(2)}, u32[]{:S(2)}) async-start(bf16[32,2,8,256]{3,2,1,0:T(8,128)(2,1)} %bitcast.17), calls=%async_computation.5 | async-start | bytes 524288 | tf_op jit(solution)/shard_map/all_to_all | solution.py:12
  242.0 28.9 %all-to-all-start.8 = ((bf16[32,8,128]{2,1,0:T(8,128)(2,1)}), bf16[32,8,128]{2,1,0:T(8,128)(2,1)S(1)}, u32[]{:S(2)}, u32[]{:S(2)}) async-start(bf16[32,8,128]{2,1,0:T(8,128)(2,1)} %fusion), calls=%async_computation.8 | async-start | bytes 131072 | tf_op jit(solution)/shard_map/all_to_all | solution.py:12

commit v2 on v1

--- a/solution.py
+++ b/solution.py
@@ -1,11 +1,16 @@
 import jax
 import jax.numpy as jnp
 from jax import lax
+from jax.sharding import Mesh
 from jax.sharding import PartitionSpec as P
+
 
 epsilon = 1e-06
 bf16 = jnp.bfloat16
 f32 = jnp.float32
+KV = ("hi", "lo")
+NEAR = ("lo", "tp")
+NEIGHBOURS = 8
 
 
 def exchange(x, axis):
@@ -42,18 +47,22 @@
     return (normed.astype(bf16), new_state)
 
 
-def mixer_weights(w_up, w_down, mixer_gain, n_kv, n_tp):
+def mixer_weights(w_up, w_down, mixer_gain):
+    near = lax.axis_size("lo")
+    me = lax.axis_index("lo")
+    block, wide = w_up.shape
+    share = wide // near
     gained = (w_up.astype(f32) * mixer_gain.astype(f32)[:, None]).astype(bf16)
-    own = gained.shape[0] // n_tp
-    wide = gained.shape[1]
-    both = jnp.stack([gained.reshape(n_tp, own, wide), w_down.T.reshape(n_tp, own, wide)], axis=1)
-    arrived = exchange(both, "tp")
-    hidden_here = wide * n_tp // n_kv
-    pieces = arrived.reshape(n_tp, 2, own, wide // hidden_here, hidden_here)
-    pieces = pieces.transpose(0, 3, 1, 2, 4).reshape(n_kv, 2, own, hidden_here)
-    whole = exchange(pieces, "kv")
-    up = whole[:, 0].reshape(n_kv * own, hidden_here)
-    down_t = whole[:, 1].reshape(n_kv * own, hidden_here)
+    both = jnp.concatenate([gained, w_down.T], axis=0)
+    both = both.reshape(2 * block, near, share).transpose(1, 0, 2)
+    whole = jnp.zeros_like(both)
+    for step in range(near):
+        piece = lax.dynamic_slice_in_dim(both, me ^ step, 1, axis=0)
+        if step:
+            piece = lax.ppermute(piece, "lo", [(i, i ^ step) for i in range(near)])
+        whole = lax.dynamic_update_slice_in_dim(whole, piece, me ^ step, axis=0)
+    up = whole[:, :block].reshape(near * block, share)
+    down_t = whole[:, block:].reshape(near * block, share)
     return up, down_t
 
 
@@ -75,12 +84,13 @@
     w_down,
 ):
     seq_here, heads_here, head_size = state.shape[:3]
-    n_kv = lax.axis_size("kv")
+    n_kv = lax.axis_size(KV)
     n_tp = lax.axis_size("tp")
+    n_near = lax.axis_size(NEAR)
     width = w_beta.shape[0]
     rows, own = tokens.shape
     block = own * n_tp
-    kv_index = lax.axis_index("kv")
+    kv_index = lax.axis_index(KV)
     tp_index = lax.axis_index("tp")
     columns = heads_here * head_size
 
@@ -99,7 +109,8 @@
         squares[:, None].astype(bf16),
     ]
     sent = jnp.concatenate(parts, axis=1).reshape(n_kv, seq_here, -1)
-    sums = exchange(sent, "kv").astype(f32).sum(axis=0)
+    arrived = exchange(sent, KV)
+    sums = arrived.astype(f32).sum(axis=0)
     first = lax.rsqrt(sums[:, -1:] / width + epsilon)
     pre = first * sums
     heads = lambda n: pre[:, n * columns : (n + 1) * columns].reshape(seq_here, heads_here, head_size)
@@ -115,49 +126,54 @@
         dt_bias,
         head_gain,
     )
-    up, down_t = mixer_weights(w_up, w_down, mixer_gain, n_kv, n_tp)
+    up, down_t = mixer_weights(w_up, w_down, mixer_gain)
 
-    every = from_everyone(normed.reshape(seq_here, columns), "kv").reshape(rows, columns)
+    every = from_everyone(normed.reshape(seq_here, columns), KV).reshape(rows, columns)
     head_part = dotted(w_out, every, 0, 1).astype(bf16)
     arrived = exchange(head_part.reshape(n_tp, own, rows), "tp")
     middle_own = (tokens_t.astype(f32) + arrived.astype(f32).sum(axis=0)).astype(bf16)
 
-    middle = from_everyone(middle_own, "kv").reshape(n_kv * own, rows)
+    middle = from_everyone(middle_own, NEAR).reshape(n_near * own, rows)
     middle_f = middle.astype(f32)
     squares_two = jnp.sum(middle_f * middle_f, axis=0, keepdims=True)
     hidden_part = dotted(up, middle, 0, 0)
     tail = jnp.broadcast_to(squares_two, (8, rows))
     sent = jnp.concatenate([hidden_part, tail], axis=0).astype(bf16)
-    sums = from_everyone(sent, "tp").astype(f32).sum(axis=0)
+    sums = from_everyone(sent, "hi").astype(f32).sum(axis=0)
     second = lax.rsqrt(sums[-1:] / width + epsilon)
     hidden = jnp.square(jax.nn.relu(second * sums[:-8])).astype(bf16)
     down_part = dotted(down_t, hidden, 1, 0).astype(bf16)
-    lowered = exchange(down_part.reshape(n_kv, own, rows), "kv").astype(f32).sum(axis=0)
+    arrived = exchange(down_part.reshape(n_near, own, rows), NEAR)
+    lowered = arrived.astype(f32).sum(axis=0)
     mixed = (middle_own.astype(f32) + lowered).astype(bf16).T
     return (mixed, new_state)
 
 
 def solution(mesh):
+    near = min(NEIGHBOURS, mesh.shape["kv"])
+    devices = mesh.devices.reshape(mesh.shape["grp"], -1, near, mesh.shape["tp"])
+    fine = Mesh(devices, ("grp", "hi", "lo", "tp"))
+    every = ("hi", "lo", "tp")
     return jax.shard_map(
         local,
-        mesh=mesh,
+        mesh=fine,
         in_specs=(
-            P("grp", ("kv", "tp")),
-            P(("grp", "kv"), "tp", None, None),
-            P("kv"),
-            P("kv", "tp"),
-            P("kv", "tp"),
-            P("kv", "tp"),
+            P("grp", every),
+            P(("grp", "hi", "lo"), "tp", None, None),
+            P(KV),
+            P(KV, "tp"),
+            P(KV, "tp"),
+            P(KV, "tp"),
             P(),
             P(),
             P("tp"),
             P("tp"),
             P(),
-            P("tp", "kv"),
-            P("kv"),
-            P("kv", "tp"),
-            P("tp", "kv"),
+            P("tp", KV),
+            P(KV),
+            P(KV, "tp"),
+            P("tp", KV),
         ),
-        out_specs=(P("grp", ("kv", "tp")), P(("grp", "kv"), "tp", None, None)),
+        out_specs=(P("grp", every), P(("grp", "hi", "lo"), "tp", None, None)),
         check_vma=False,
     )

time: 273 us -> 246 us (0.901)
  waiting for transfers between devices: 155 us -> 81.9 us
  starting transfers between devices: 81.7 us -> 114 us
  blocking collectives: 18.5 us -> 29.3 us
  local copies, waits for them, and re-layouts: 6.15 us -> 12.4 us
    all_to_all x8 -> x6, waiting for transfers between devices: 155 us -> 73.7 us  [exchange(): return lax.all_to_all(x, axis, split_axis=0, concat_axis=0, tiled=True)]
    ppermute x0 -> x7, starting transfers between devices: none -> 30.3 us  [mixer_weights(): piece = lax.ppermute(piece, 'lo', [(i, i ^ step) for i in range(near)])]
    all_to_all x1, blocking collectives: 18.5 us -> 29.3 us  [exchange(): return lax.all_to_all(x, axis, split_axis=0, concat_axis=0, tiled=True)]
    ppermute x0 -> x7, waiting for transfers between devices: none -> 8.16 us  [mixer_weights(): piece = lax.ppermute(piece, 'lo', [(i, i ^ step) for i in range(near)])]
    unnamed x22 -> x26, local copies, waits for them, and re-layouts: 0.05 us -> 5.05 us
    all_to_all x8 -> x6, starting transfers between devices: 81.7 us -> 83.7 us  [exchange(): return lax.all_to_all(x, axis, split_axis=0, concat_axis=0, tiled=True)]
  transfers between devices with their start and end apart: 8 -> 13, of which waited for: 8 -> 5; matrix products, arithmetic and copies ran while one was open for 2% -> 2% of each run, Pallas kernels for 0% -> 0%
where the time goes in v2:
time: 246 us; the launch traced here: 245 us
  starting transfers between devices  114 us (46%)
  waiting for transfers between devices  81.9 us (33%)
  blocking collectives  29.3 us (12%)
  local copies, waits for them, and re-layouts  12.4 us (5%)
  matrix products  3.17 us (1%)
  other arithmetic  2.99 us (1%)
    all_to_all x6, starting transfers between devices, exchange(): return lax.all_to_all(x, axis, split_axis=0, concat_axis=0, tiled=True)  83.7 us
    all_to_all x6, waiting for transfers between devices, exchange(): return lax.all_to_all(x, axis, split_axis=0, concat_axis=0, tiled=True)  73.7 us
    ppermute x7, starting transfers between devices, mixer_weights(): piece = lax.ppermute(piece, 'lo', [(i, i ^ step) for i in range(near)])  30.3 us
    all_to_all x1, blocking collectives, exchange(): return lax.all_to_all(x, axis, split_axis=0, concat_axis=0, tiled=True)  29.3 us
    ppermute x7, waiting for transfers between devices, mixer_weights(): piece = lax.ppermute(piece, 'lo', [(i, i ^ step) for i in range(near)])  8.16 us
    unnamed x26, local copies, waits for them, and re-layouts  5.05 us
  transfers between devices with their start and end apart: 13, of which 5 were waited for; matrix products, arithmetic and copies ran while one was open for 2% of the time, Pallas kernels for 0%

profile of v2, /device:TPU:33, one launch (start us, length us, event | category | flops | bytes accessed | tf_op | source)
XLA Modules:
  0.0 244.8 jit_solution(9004266843202391231)
XLA Ops:
  0.6 1.3 broadcast_in_dim.12
  1.9 44.7 %all-to-all-start = ((bf16[8,8,128]{2,1,0:T(8,128)(2,1)}), bf16[8,8,128]{2,1,0:T(8,128)(2,1)S(1)}, u32[]{:S(2)}, u32[]{:S(2)}) async-start(bf16[8,8,128]{2,1,0:T(8,128)(2,1)} %broadcast_in_dim.12), calls=%async_computation | async-start | bytes 32768 | tf_op jit(solution)/shard_map/all_to_all | solution.py:17
  46.6 0.7 copy-done.10
  47.3 0.8 dynamic_slice.31
  48.0 0.8 dynamic_slice.30
  48.8 2.5 %all-to-all-done = bf16[8,8,128]{2,1,0:T(8,128)(2,1)S(1)} async-done(((bf16[8,8,128]{2,1,0:T(8,128)(2,1)}), bf16[8,8,128]{2,1,0:T(8,128)(2,1)S(1)}, u32[]{:S(2)}, u32[]{:S(2)}) %all-to-all-start) | async-done | bytes 16416 | tf_op jit(solution)/shard_map/all_to_all | solution.py:17
  51.3 0.3 convolution_convert_fusion.3
  51.6 0.7 copy-done.4
  52.4 0.3 convolution_convert_fusion.2
  52.7 0.7 copy-done.5
  53.4 0.3 convolution_convert_fusion.1
  53.7 0.2 convolution_convert_fusion.6
  53.9 0.1 copy.141
  54.1 0.2 convert_element_type.134
  54.3 0.9 concatenate.27
  55.2 6.9 %all-to-all-start.1 = ((bf16[32,4,773]{2,1,0:T(4,128)(2,1)}), bf16[32,4,773]{2,1,0:T(4,128)(2,1)S(1)}, u32[]{:S(2)}, u32[]{:S(2)}) async-start(bf16[32,4,773]{2,1,0:T(4,128)(2,1)} %concatenate.27), calls=%async_computation.1 | async-start | bytes 458752 | tf_op jit(solution)/shard_map/all_to_all | solution.py:17
  62.2 37.3 %all-to-all-done.1 = bf16[32,4,773]{2,1,0:T(4,128)(2,1)S(1)} async-done(((bf16[32,4,773]{2,1,0:T(4,128)(2,1)}), bf16[32,4,773]{2,1,0:T(4,128)(2,1)S(1)}, u32[]{:S(2)}, u32[]{:S(2)}) %all-to-all-start.1) | async-done | bytes 197920 | tf_op jit(solution)/shard_map/all_to_all | solution.py:17
  99.5 0.1 convert_reduce_fusion
  99.6 0.2 fusion.25
  100.1 0.2 multiply_reduce_fusion.2
  100.3 0.1 copy.123
  100.4 0.6 copy-done.9
  101.0 0.1 copy.122
  101.1 0.2 fusion.41
  101.3 0.2 fusion.42
  101.5 0.1 copy.124
  101.6 0.2 multiply_reduce_fusion.1
  101.7 0.1 copy.125
  101.8 0.1 copy.126
  101.9 0.2 copy-done.8
  102.2 0.7 broadcast_in_dim.13
  102.9 4.8 %all-to-all-start.2 = ((bf16[32,4,256]{2,1,0:T(4,128)(2,1)}), bf16[32,4,256]{2,1,0:T(4,128)(2,1)S(1)}, u32[]{:S(2)}, u32[]{:S(2)}) async-start(bf16[32,4,256]{2,1,0:T(4,128)(2,1)} %broadcast_in_dim.13), calls=%async_computation.2 | async-start | bytes 131072 | tf_op jit(solution)/shard_map/all_to_all | solution.py:17
  107.7 0.6 copy-done.12
  108.4 0.8 copy-done.3
  109.3 0.2 copy.127
  109.5 20.7 %all-to-all-done.2 = bf16[32,4,256]{2,1,0:T(4,128)(2,1)S(1)} async-done(((bf16[32,4,256]{2,1,0:T(4,128)(2,1)}), bf16[32,4,256]{2,1,0:T(4,128)(2,1)S(1)}, u32[]{:S(2)}, u32[]{:S(2)}) %all-to-all-start.2) | async-done | bytes 65568 | tf_op jit(solution)/shard_map/all_to_all | solution.py:17
  130.3 0.8 fusion.1
  131.0 7.0 %all-to-all-start.3 = ((bf16[8,8,128]{2,1,0:T(8,128)(2,1)}), bf16[8,8,128]{2,1,0:T(8,128)(2,1)S(1)}, u32[]{:S(2)}, u32[]{:S(2)}) async-start(bf16[8,8,128]{2,1,0:T(8,128)(2,1)} %fusion.1), calls=%async_computation.3 | async-start | bytes 32768 | tf_op jit(solution)/shard_map/all_to_all | solution.py:17
  138.1 0.1 copy.129
  138.2 2.2 collective-permute-start
  140.4 0.1 copy.130
  140.5 2.1 collective-permute-start.1
  142.7 0.1 copy.131
  142.8 5.0 %collective-permute-start.2 = (bf16[1,128,128]{2,1,0:T(8,128)(2,1)S(1)}, bf16[1,128,128]{2,1,0:T(8,128)(2,1)S(1)}, u32[]{:S(2)}, u32[]{:S(2)}) collective-permute-start(bf16[1,128,128]{2,1,0:T(8,128)(2,1)S(1)} %bitcast.94), channel_id=1, source_target_pairs={{0,24},{8,16},{16,8},{24,0},{32,56},{40,48},{48,40},{56,32},{1,25}... | collective-permute-start | bytes 98312 | tf_op jit(solution)/shard_map/ppermute | solution.py:62
  147.8 0.1 copy.132
  147.9 2.0 collective-permute-start.3
  149.9 0.1 copy.133
  150.0 6.4 %collective-permute-start.4 = (bf16[1,128,128]{2,1,0:T(8,128)(2,1)S(1)}, bf16[1,128,128]{2,1,0:T(8,128)(2,1)S(1)}, u32[]{:S(2)}, u32[]{:S(2)}) collective-permute-start(bf16[1,128,128]{2,1,0:T(8,128)(2,1)S(1)} %bitcast.92), channel_id=1, source_target_pairs={{0,40},{8,32},{16,56},{24,48},{32,8},{40,0},{48,24},{56,16},{1,41}... | collective-permute-start | bytes 98312 | tf_op jit(solution)/shard_map/ppermute | solution.py:62
  156.4 0.1 copy.128
  156.5 0.7 copy-done.7
  157.2 0.7 broadcast_in_dim.15
  157.9 8.9 %all-to-all-start.4 = ((bf16[64,8,128]{2,1,0:T(8,128)(2,1)}), bf16[64,8,128]{2,1,0:T(8,128)(2,1)S(1)}, u32[]{:S(2)}, u32[]{:S(2)}) async-start(bf16[64,8,128]{2,1,0:T(8,128)(2,1)} %broadcast_in_dim.15), calls=%async_computation.4 | async-start | bytes 262144 | tf_op jit(solution)/shard_map/all_to_all | solution.py:17
  166.8 0.1 copy.134
  166.9 0.1 copy.135
  167.1 9.6 %collective-permute-start.5 = (bf16[1,128,128]{2,1,0:T(8,128)(2,1)S(1)}, bf16[1,128,128]{2,1,0:T(8,128)(2,1)S(1)}, u32[]{:S(2)}, u32[]{:S(2)}) collective-permute-start(bf16[1,128,128]{2,1,0:T(8,128)(2,1)S(1)} %bitcast.98), channel_id=1, source_target_pairs={{0,48},{8,56},{16,32},{24,40},{32,16},{40,24},{48,0},{56,8},{1,49}... | collective-permute-start | bytes 98312 | tf_op jit(solution)/shard_map/ppermute | solution.py:62
  176.7 3.0 %collective-permute-start.6 = (bf16[1,128,128]{2,1,0:T(8,128)(2,1)S(1)}, bf16[1,128,128]{2,1,0:T(8,128)(2,1)S(1)}, u32[]{:S(2)}, u32[]{:S(2)}) collective-permute-start(bf16[1,128,128]{2,1,0:T(8,128)(2,1)S(1)} %bitcast.97), channel_id=1, source_target_pairs={{0,56},{8,48},{16,40},{24,32},{32,24},{40,16},{48,8},{56,0},{1,57}... | collective-permute-start | bytes 98312 | tf_op jit(solution)/shard_map/ppermute | solution.py:62
  179.9 8.1 %collective-permute-done.6 = bf16[1,128,128]{2,1,0:T(8,128)(2,1)S(1)} collective-permute-done((bf16[1,128,128]{2,1,0:T(8,128)(2,1)S(1)}, bf16[1,128,128]{2,1,0:T(8,128)(2,1)S(1)}, u32[]{:S(2)}, u32[]{:S(2)}) %collective-permute-start.6) | collective-permute-done | bytes 32800 | tf_op jit(solution)/shard_map/ppermute | solution.py:62
  188.1 0.2 convolution_convert_fusion.4
  188.4 29.3 %all_to_all.35 = bf16[4,136,128]{2,1,0:T(8,128)(2,1)S(1)} all-to-all(bf16[4,136,128]{2,1,0:T(8,128)(2,1)S(1)} %broadcast_in_dim.17), channel_id=1, replica_groups=mesh['grp'=2,'hi'=4,'lo'=8,'tp'=8] {'hi'}, dimensions={0} | all-to-all | bytes 278528 | tf_op jit(solution)/shard_map/all_to_all | solution.py:17
  217.7 0.8 fusion
  218.6 11.5 %all-to-all-start.6 = ((bf16[64,8,128]{2,1,0:T(8,128)(2,1)}), bf16[64,8,128]{2,1,0:T(8,128)(2,1)S(1)}, u32[]{:S(2)}, u32[]{:S(2)}) async-start(bf16[64,8,128]{2,1,0:T(8,128)(2,1)} %fusion), calls=%async_computation.6 | async-start | bytes 262144 | tf_op jit(solution)/shard_map/all_to_all | solution.py:17
  230.0 1.0 multiply_add_fusion
  231.0 13.1 %all-to-all-done.6 = bf16[64,8,128]{2,1,0:T(8,128)(2,1)S(1)} async-done(((bf16[64,8,128]{2,1,0:T(8,128)(2,1)}), bf16[64,8,128]{2,1,0:T(8,128)(2,1)S(1)}, u32[]{:S(2)}, u32[]{:S(2)}) %all-to-all-start.6) | async-done | bytes 131104 | tf_op jit(solution)/shard_map/all_to_all | solution.py:17
  244.2 0.6 fusion.14
  (67 shorter events, 1.2 us)
Async XLA Ops:
  0.6 50.7 %copy-start = (bf16[64,256]{1,0:T(8,128)(2,1)S(1)}, bf16[64,256]{1,0:T(8,128)(2,1)}, u32[]{:S(2)}) copy-start(bf16[64,256]{1,0:T(8,128)(2,1)} %param.18) | copy-start | bytes 98308
  1.9 49.4 %all-to-all-start = ((bf16[8,8,128]{2,1,0:T(8,128)(2,1)}), bf16[8,8,128]{2,1,0:T(8,128)(2,1)S(1)}, u32[]{:S(2)}, u32[]{:S(2)}) async-start(bf16[8,8,128]{2,1,0:T(8,128)(2,1)} %broadcast_in_dim.12), calls=%async_computation | async-start | bytes 32768 | tf_op jit(solution)/shard_map/all_to_all | solution.py:17
  46.6 0.7 copy-start.10
  51.6 0.8 copy-start.4
  52.6 0.8 copy-start.5
  54.3 7.8 %copy-start.11 = (f32[2]{0:T(128)S(1)}, f32[2]{0:T(128)}, u32[]{:S(2)}) copy-start(f32[2]{0:T(128)} %param.23) | copy-start | bytes 28
  55.2 45.9 %copy-start.1 = (f32[4,2,128,128]{3,2,1,0:T(8,128)S(1)}, f32[4,2,128,128]{3,2,1,0:T(8,128)}, u32[]{:S(2)}) copy-start(f32[4,2,128,128]{3,2,1,0:T(8,128)} %param.16) | copy-start | bytes 1572868
  55.2 44.3 %all-to-all-start.1 = ((bf16[32,4,773]{2,1,0:T(4,128)(2,1)}), bf16[32,4,773]{2,1,0:T(4,128)(2,1)S(1)}, u32[]{:S(2)}, u32[]{:S(2)}) async-start(bf16[32,4,773]{2,1,0:T(4,128)(2,1)} %concatenate.27), calls=%async_computation.1 | async-start | bytes 458752 | tf_op jit(solution)/shard_map/all_to_all | solution.py:17
  100.3 0.7 copy-start.9
  101.5 0.7 copy-start.8
  101.9 6.4 %copy-start.2 = (bf16[64,1024]{1,0:T(8,128)(2,1)S(1)}, bf16[64,1024]{1,0:T(8,128)(2,1)}, u32[]{:S(2)}) copy-start(bf16[64,1024]{1,0:T(8,128)(2,1)} %param.28) | copy-start | bytes 393220
  102.9 27.4 %all-to-all-start.2 = ((bf16[32,4,256]{2,1,0:T(4,128)(2,1)}), bf16[32,4,256]{2,1,0:T(4,128)(2,1)S(1)}, u32[]{:S(2)}, u32[]{:S(2)}) async-start(bf16[32,4,256]{2,1,0:T(4,128)(2,1)} %broadcast_in_dim.13), calls=%async_computation.2 | async-start | bytes 131072 | tf_op jit(solution)/shard_map/all_to_all | solution.py:17
  107.7 0.7 copy-start.12
  108.4 0.9 copy-start.3
  109.5 20.8 %copy-start.6 = (bf16[256,64]{0,1:T(8,128)(2,1)S(1)}, bf16[256,64]{0,1:T(8,128)(2,1)}, u32[]{:S(2)}) copy-start(bf16[256,64]{0,1:T(8,128)(2,1)} %param.26) | copy-start | bytes 98308
  131.0 25.5 %all-to-all-start.3 = ((bf16[8,8,128]{2,1,0:T(8,128)(2,1)}), bf16[8,8,128]{2,1,0:T(8,128)(2,1)S(1)}, u32[]{:S(2)}, u32[]{:S(2)}) async-start(bf16[8,8,128]{2,1,0:T(8,128)(2,1)} %fusion.1), calls=%async_computation.3 | async-start | bytes 32768 | tf_op jit(solution)/shard_map/all_to_all | solution.py:17
  138.2 28.9 %collective-permute-start = (bf16[1,128,128]{2,1,0:T(8,128)(2,1)S(1)}, bf16[1,128,128]{2,1,0:T(8,128)(2,1)S(1)}, u32[]{:S(2)}, u32[]{:S(2)}) collective-permute-start(bf16[1,128,128]{2,1,0:T(8,128)(2,1)S(1)} %bitcast.96), channel_id=1, source_target_pairs={{0,8},{8,0},{16,24},{24,16},{32,40},{40,32},{48,56},{56,48},{1,9},... | collective-permute-start | bytes 98312 | tf_op jit(solution)/shard_map/ppermute | solution.py:62
  140.5 36.2 %collective-permute-start.1 = (bf16[1,128,128]{2,1,0:T(8,128)(2,1)S(1)}, bf16[1,128,128]{2,1,0:T(8,128)(2,1)S(1)}, u32[]{:S(2)}, u32[]{:S(2)}) collective-permute-start(bf16[1,128,128]{2,1,0:T(8,128)(2,1)S(1)} %bitcast.95), channel_id=1, source_target_pairs={{0,16},{8,24},{16,0},{24,8},{32,48},{40,56},{48,32},{56,40},{1,17}... | collective-permute-start | bytes 98312 | tf_op jit(solution)/shard_map/ppermute | solution.py:62
  142.8 37.0 %collective-permute-start.2 = (bf16[1,128,128]{2,1,0:T(8,128)(2,1)S(1)}, bf16[1,128,128]{2,1,0:T(8,128)(2,1)S(1)}, u32[]{:S(2)}, u32[]{:S(2)}) collective-permute-start(bf16[1,128,128]{2,1,0:T(8,128)(2,1)S(1)} %bitcast.94), channel_id=1, source_target_pairs={{0,24},{8,16},{16,8},{24,0},{32,56},{40,48},{48,40},{56,32},{1,25}... | collective-permute-start | bytes 98312 | tf_op jit(solution)/shard_map/ppermute | solution.py:62
  147.9 31.8 %collective-permute-start.3 = (bf16[1,128,128]{2,1,0:T(8,128)(2,1)S(1)}, bf16[1,128,128]{2,1,0:T(8,128)(2,1)S(1)}, u32[]{:S(2)}, u32[]{:S(2)}) collective-permute-start(bf16[1,128,128]{2,1,0:T(8,128)(2,1)S(1)} %bitcast.93), channel_id=1, source_target_pairs={{0,32},{8,40},{16,48},{24,56},{32,0},{40,8},{48,16},{56,24},{1,33}... | collective-permute-start | bytes 98312 | tf_op jit(solution)/shard_map/ppermute | solution.py:62
  150.0 29.8 %collective-permute-start.4 = (bf16[1,128,128]{2,1,0:T(8,128)(2,1)S(1)}, bf16[1,128,128]{2,1,0:T(8,128)(2,1)S(1)}, u32[]{:S(2)}, u32[]{:S(2)}) collective-permute-start(bf16[1,128,128]{2,1,0:T(8,128)(2,1)S(1)} %bitcast.92), channel_id=1, source_target_pairs={{0,40},{8,32},{16,56},{24,48},{32,8},{40,0},{48,24},{56,16},{1,41}... | collective-permute-start | bytes 98312 | tf_op jit(solution)/shard_map/ppermute | solution.py:62
  156.5 0.7 copy-start.7
  157.9 30.2 %all-to-all-start.4 = ((bf16[64,8,128]{2,1,0:T(8,128)(2,1)}), bf16[64,8,128]{2,1,0:T(8,128)(2,1)S(1)}, u32[]{:S(2)}, u32[]{:S(2)}) async-start(bf16[64,8,128]{2,1,0:T(8,128)(2,1)} %broadcast_in_dim.15), calls=%async_computation.4 | async-start | bytes 262144 | tf_op jit(solution)/shard_map/all_to_all | solution.py:17
  167.1 12.8 %collective-permute-start.5 = (bf16[1,128,128]{2,1,0:T(8,128)(2,1)S(1)}, bf16[1,128,128]{2,1,0:T(8,128)(2,1)S(1)}, u32[]{:S(2)}, u32[]{:S(2)}) collective-permute-start(bf16[1,128,128]{2,1,0:T(8,128)(2,1)S(1)} %bitcast.98), channel_id=1, source_target_pairs={{0,48},{8,56},{16,32},{24,40},{32,16},{40,24},{48,0},{56,8},{1,49}... | collective-permute-start | bytes 98312 | tf_op jit(solution)/shard_map/ppermute | solution.py:62
  176.7 11.3 %collective-permute-start.6 = (bf16[1,128,128]{2,1,0:T(8,128)(2,1)S(1)}, bf16[1,128,128]{2,1,0:T(8,128)(2,1)S(1)}, u32[]{:S(2)}, u32[]{:S(2)}) collective-permute-start(bf16[1,128,128]{2,1,0:T(8,128)(2,1)S(1)} %bitcast.97), channel_id=1, source_target_pairs={{0,56},{8,48},{16,40},{24,32},{32,24},{40,16},{48,8},{56,0},{1,57}... | collective-permute-start | bytes 98312 | tf_op jit(solution)/shard_map/ppermute | solution.py:62
  218.6 25.6 %all-to-all-start.6 = ((bf16[64,8,128]{2,1,0:T(8,128)(2,1)}), bf16[64,8,128]{2,1,0:T(8,128)(2,1)S(1)}, u32[]{:S(2)}, u32[]{:S(2)}) async-start(bf16[64,8,128]{2,1,0:T(8,128)(2,1)} %fusion), calls=%async_computation.6 | async-start | bytes 262144 | tf_op jit(solution)/shard_map/all_to_all | solution.py:17
